TPU v7x, 256 devices: a whole 4x4x8 slice. The times are simulated.
256 devices in a mesh: rep: 2 (over z_hi), fs: 16 (over z_lo, x), tp: 8 (over y, core).
Axes of the slice: x: 4, y: 4, z: 8 (z_hi: 2, z_lo: 4; z = z_hi * 4 + z_lo), core: 2. Of those that a mesh axis runs over, the one named last changes fastest.
Arguments:
- tokens: bfloat16 [32768, 2048], P(('rep', 'fs'), 'tp'), may hold values from -6 to 6
- mix_in_gain: bfloat16 [2048], replicated, may hold values from 0.099609375 to 1.8984375
- bgate_weight: bfloat16 [2048, 2048], P('fs', 'tp'), may hold values from -0.125 to 0.125
- cgate_weight: bfloat16 [2048, 2048], P('fs', 'tp'), may hold values from -0.125 to 0.125
- value_weight: bfloat16 [2048, 2048], P('fs', 'tp'), may hold values from -0.125 to 0.125
- conv_taps: bfloat16 [3, 2048], replicated, may hold values from -3 to 3
- out_weight: bfloat16 [2048, 2048], P('tp', 'fs'), may hold values from -0.41984465 to 0.41984465
- mix_out_gain: bfloat16 [2048], replicated, may hold values from 0.099609375 to 1.8984375
- ffn_in_gain: bfloat16 [2048], replicated, may hold values from 0.099609375 to 1.8984375
- up_weight: bfloat16 [2048, 8192], P('fs', 'tp'), may hold values from -0.125 to 0.125
- down_weight: bfloat16 [8192, 2048], P('tp', 'fs'), may hold values from -0.20992233 to 0.20992233
- ffn_out_gain: bfloat16 [2048], replicated, may hold values from 0.099609375 to 1.8984375
Outputs:
- result: bfloat16 [32768, 2048], P(('rep', 'fs'), 'tp')
All inputs are finite; a program needn't handle non-finite values.
Results may differ from a plain program's by a relative error of at most 0.02.
Values may be sent and summed in bfloat16 or wider, within the bound.
A program may use at most 128 MiB of HBM per device.

v0:
```python
import jax
import jax.numpy as jnp
from jax import lax
from jax.sharding import Mesh
from jax.sharding import PartitionSpec as P

LEN = 256
FS = ("fs_0", "fs_1")
REP_FS = ("rep", "fs_0", "fs_1")
epsilon = 1e-06


def in_order(pieces, dim):
    pieces = jnp.moveaxis(pieces, 0, dim)
    shape = pieces.shape
    return pieces.reshape(*shape[:dim], shape[dim] * shape[dim + 1], *shape[dim + 2 :])


def from_everyone(x, axis):
    length = lax.axis_size(axis)
    return lax.all_to_all(jnp.broadcast_to(x[None], (length, *x.shape)), axis, 0, 0, tiled=True)


def gathered_copies(x, axis, dim):
    return in_order(from_everyone(x, axis), dim)


def in_blocks(x, dim, length):
    before, after = (x.shape[:dim], x.shape[dim + 1 :])
    return jnp.moveaxis(x.reshape(*before, length, -1, *after), dim, 0)


def sent_and_summed(x, axis, dim):
    pieces = in_blocks(x, dim, lax.axis_size(axis))
    arrived = lax.all_to_all(pieces, axis, split_axis=0, concat_axis=0, tiled=True)
    return arrived.astype(jnp.float32).sum(axis=0)


def of_everyone(x, axis):
    everything = from_everyone(x, axis)
    return jnp.sum(everything, axis=0)


def all_blocks(x, axes, order):
    pieces = x
    for k in order:
        pieces = lax.all_gather(pieces, axes[k])
    done = order[::-1]
    back = [done.index(k) for k in range(len(axes))]
    pieces = pieces.transpose(*back, *range(len(axes), pieces.ndim))
    return pieces.reshape(-1, *x.shape)


def whole_of(x, axes, order, dim):
    return in_order(all_blocks(x, axes, order), dim)


def normalize(rows, gain):
    rows = rows.astype(jnp.float32)
    factor = lax.rsqrt(jnp.mean(rows * rows, axis=-1, keepdims=True) + epsilon)
    return rows * factor * gain.astype(jnp.float32)


def convolve(inner, taps):
    seqs = inner.reshape(-1, LEN, inner.shape[1])
    padded = jnp.pad(seqs, ((0, 0), (1, 1), (0, 0)))
    weights = taps.astype(jnp.float32)
    out = weights[0] * padded[:, :-2] + weights[1] * padded[:, 1:-1] + weights[2] * padded[:, 2:]
    return out.reshape(inner.shape)


def body(
    tokens,
    mix_in_gain,
    bgate_weight,
    cgate_weight,
    value_weight,
    conv_taps,
    out_weight,
    mix_out_gain,
    ffn_in_gain,
    up_weight,
    down_weight,
    ffn_out_gain,
):
    column = lax.axis_index("tp")
    own_width = tokens.shape[1]
    first = column * own_width
    full_width = mix_in_gain.shape[0]
    whole = lax.all_gather(tokens, "tp", axis=1, tiled=True)
    normed = normalize(whole, mix_in_gain).astype(jnp.bfloat16)

    def add_rows(piece):
        return jnp.dot(normed, piece, preferred_element_type=jnp.float32)

    bgate = add_rows(gathered_copies(bgate_weight, FS, 0))
    cgate = add_rows(gathered_copies(cgate_weight, FS, 0))
    value = add_rows(gathered_copies(value_weight, FS, 0))
    bgate = bgate.astype(jnp.bfloat16)
    cgate = cgate.astype(jnp.bfloat16)
    value = value.astype(jnp.bfloat16)
    channels = bgate.shape[1]
    own_taps = lax.dynamic_slice_in_dim(conv_taps, column * channels, channels, 1)
    inner = cgate.astype(jnp.float32) * value.astype(jnp.float32)
    gated = (bgate.astype(jnp.float32) * convolve(inner, own_taps)).astype(jnp.bfloat16)
    partial_mix = jnp.dot(
        gated, gathered_copies(out_weight, FS, 1), preferred_element_type=jnp.float32
    )
    mixed = sent_and_summed(partial_mix.astype(jnp.bfloat16), "tp", 1)
    power = of_everyone(jnp.sum(mixed * mixed, axis=1), "tp")
    gain_own = lax.dynamic_slice_in_dim(mix_out_gain, first, own_width, 0).astype(jnp.float32)
    scaled = mixed * lax.rsqrt(power[:, None] / full_width + epsilon) * gain_own
    resid_own = (tokens.astype(jnp.float32) + scaled).astype(jnp.bfloat16)
    resid = lax.all_gather(resid_own, "tp", axis=1, tiled=True)
    second = normalize(resid, ffn_in_gain).astype(jnp.bfloat16)
    lifted = jnp.dot(second, whole_of(up_weight, FS, (0, 1), 0), preferred_element_type=jnp.float32)
    active = jnp.square(jnp.maximum(lifted, 0.0)).astype(jnp.bfloat16)
    partial_ffn = jnp.dot(
        active, whole_of(down_weight, FS, (0, 1), 1), preferred_element_type=jnp.float32
    )
    ffn = sent_and_summed(partial_ffn.astype(jnp.bfloat16), "tp", 1)
    ffn_energy = of_everyone(jnp.sum(ffn * ffn, axis=1), "tp")
    out_gain = lax.dynamic_slice_in_dim(ffn_out_gain, first, own_width, 0).astype(jnp.float32)
    closing = ffn * lax.rsqrt(ffn_energy[:, None] / full_width + epsilon) * out_gain
    return (resid_own.astype(jnp.float32) + closing).astype(jnp.bfloat16)


def solution(mesh):
    torus = Mesh(
        mesh.devices.reshape(mesh.shape["rep"], 4, 4, mesh.shape["tp"]),
        ("rep", "fs_0", "fs_1", "tp"),
    )
    return jax.shard_map(
        body,
        mesh=torus,
        in_specs=(
            P(REP_FS, "tp"),
            P(),
            P(FS, "tp"),
            P(FS, "tp"),
            P(FS, "tp"),
            P(),
            P("tp", FS),
            P(),
            P(),
            P(FS, "tp"),
            P("tp", FS),
            P(),
        ),
        out_specs=P(REP_FS, "tp"),
        check_vma=False,
    )
```

profile of v0, /device:TPU:1, one launch (start us, length us, event | category | flops | bytes accessed | tf_op | source)
XLA Modules:
  0.0 391.8 jit_solution(6726258593251835402)
XLA Ops:
  6.5 0.7 all-gather.19.cloned.1.call-update
  7.3 0.7 all-gather.15.cloned.1.call-update
  8.1 0.7 all-gather.11.cloned.1.call-update
  8.8 36.9 %all-gather.19.cloned.1.call-done = bf16[4096,128]{1,0:T(8,128)(2,1)} async-done(((bf16[1024,128]{1,0:T(8,128)(2,1)}), bf16[4096,128]{1,0:T(8,128)(2,1)}) %all-gather.19.cloned.1.call-update) | async-done | bytes 1048592 | tf_op jit(solution)/shard_map/all_gather | solution.py:47
  45.8 0.9 broadcast_in_dim.13
  46.7 40.9 %all_to_all.42 = bf16[16,128,256]{2,1,0:T(8,128)(2,1)S(1)} all-to-all(bf16[16,128,256]{2,1,0:T(8,128)(2,1)S(1)} %broadcast_in_dim.13), channel_id=1, replica_groups=mesh['rep'=2,'fs_0'=4,'fs_1'=4,'tp'=8] {'fs_0','fs_1'}, dimensions={0} | all-to-all | bytes 2097152 | tf_op jit(solution)/shard_map/all_to_all | solution.py:21
  87.6 1.1 broadcast_in_dim.14
  88.7 9.8 %all-to-all-start.2 = ((bf16[16,128,256]{2,1,0:T(8,128)(2,1)}), bf16[16,128,256]{2,1,0:T(8,128)(2,1)S(1)}, u32[]{:S(2)}, u32[]{:S(2)}) async-start(bf16[16,128,256]{2,1,0:T(8,128)(2,1)} %broadcast_in_dim.14), calls=%async_computation.2 | async-start | bytes 2097152 | tf_op jit(solution)/shard_map/all_to_all | solution.py:21
  98.5 0.1 copy.31
  98.6 21.9 %all-to-all-done.2 = bf16[16,128,256]{2,1,0:T(8,128)(2,1)S(1)} async-done(((bf16[16,128,256]{2,1,0:T(8,128)(2,1)}), bf16[16,128,256]{2,1,0:T(8,128)(2,1)S(1)}, u32[]{:S(2)}, u32[]{:S(2)}) %all-to-all-start.2) | async-done | bytes 1048608 | tf_op jit(solution)/shard_map/all_to_all | solution.py:21
  120.5 1.1 broadcast_in_dim.15
  121.5 7.9 %all-to-all-start.3 = ((bf16[16,256,128]{1,2,0:T(8,128)(2,1)}), bf16[16,256,128]{1,2,0:T(8,128)(2,1)S(1)}, u32[]{:S(2)}, u32[]{:S(2)}) async-start(bf16[16,256,128]{1,2,0:T(8,128)(2,1)} %broadcast_in_dim.15), calls=%async_computation.3 | async-start | bytes 2097152 | tf_op jit(solution)/shard_map/all_to_all | solution.py:21
  129.4 0.7 dynamic-slice_convert_fusion
  130.1 21.5 %all-to-all-done.3 = bf16[16,256,128]{1,2,0:T(8,128)(2,1)S(1)} async-done(((bf16[16,256,128]{1,2,0:T(8,128)(2,1)}), bf16[16,256,128]{1,2,0:T(8,128)(2,1)S(1)}, u32[]{:S(2)}, u32[]{:S(2)}) %all-to-all-start.3) | async-done | bytes 1048608 | tf_op jit(solution)/shard_map/all_to_all | solution.py:21
  151.6 1.2 broadcast_in_dim.12
  152.8 7.8 %all-to-all-start = ((bf16[16,128,256]{2,1,0:T(8,128)(2,1)}), bf16[16,128,256]{2,1,0:T(8,128)(2,1)}, u32[]{:S(2)}, u32[]{:S(2)}) async-start(bf16[16,128,256]{2,1,0:T(8,128)(2,1)} %broadcast_in_dim.12), calls=%async_computation | async-start | bytes 2097152 | tf_op jit(solution)/shard_map/all_to_all | solution.py:21
  160.7 0.5 all-gather.17.cloned.1.call-update
  161.2 3.2 fusion
  164.5 0.3 copy-done.1
  164.7 1.3 fusion.13
  166.0 1.3 fusion.12
  167.4 0.3 multiply_add_fusion
  167.7 15.1 %all-to-all-done = bf16[16,128,256]{2,1,0:T(8,128)(2,1)} async-done(((bf16[16,128,256]{2,1,0:T(8,128)(2,1)}), bf16[16,128,256]{2,1,0:T(8,128)(2,1)}, u32[]{:S(2)}, u32[]{:S(2)}) %all-to-all-start) | async-done | bytes 1048608 | tf_op jit(solution)/shard_map/all_to_all | solution.py:21
  182.8 8.8 %convolution_convert_fusion = bf16[1024,2048]{1,0:T(8,128)(2,1)} fusion(bf16[256,2048]{0,1:T(8,128)(2,1)S(1)} %bitcast.55, f32[1024,256]{1,0:T(8,128)S(1)} %bitcast.58, bf16[2048,256]{1,0:T(8,128)(2,1)} %bitcast, bf16[1024,2048]{1,0:T(8,128)(2,1)} %all-gather.11.cloned.1.call-done, f32[2048]{0:T(1024)S(1)} %convert_element_type.79, ...), kind=kOutput, calls=%fused_computation.18 | convolution fusion | flops 2159017984 | bytes 11546624 | tf_op jit(solution)/shard_map/dot_general | solution.py:106
  191.7 2.5 copy.46
  194.1 56.0 %all_to_all.43 = bf16[8,1024,256]{2,1,0:T(8,128)(2,1)S(1)} all-to-all(bf16[8,1024,256]{2,1,0:T(8,128)(2,1)S(1)} %bitcast.44), channel_id=1, replica_groups=mesh['rep'=2,'fs_0'=4,'fs_1'=4,'tp'=8] {'tp'}, dimensions={0} | all-to-all | bytes 8388608 | tf_op jit(solution)/shard_map/all_to_all | solution.py:35
  250.2 0.6 convert_reduce_fusion.1
  250.8 0.2 multiply_reduce_fusion.1
  251.0 0.6 broadcast_in_dim.16
  251.6 4.2 %all-to-all-start.5 = ((f32[8,1,1024]{2,1,0:T(1,128)}), f32[8,1,1024]{2,1,0:T(1,128)S(1)}, u32[]{:S(2)}, u32[]{:S(2)}) async-start(f32[8,1,1024]{2,1,0:T(1,128)} %broadcast_in_dim.16), calls=%async_computation.5 | async-start | bytes 65536 | tf_op jit(solution)/shard_map/all_to_all | solution.py:21
  255.8 0.8 dynamic-slice_convert_fusion.2
  256.6 4.0 %all-to-all-done.5 = f32[8,1,1024]{2,1,0:T(1,128)S(1)} async-done(((f32[8,1,1024]{2,1,0:T(1,128)}), f32[8,1,1024]{2,1,0:T(1,128)S(1)}, u32[]{:S(2)}, u32[]{:S(2)}) %all-to-all-start.5) | async-done | bytes 32800 | tf_op jit(solution)/shard_map/all_to_all | solution.py:21
  260.6 1.1 add_convert_fusion.1
  261.8 4.5 %copy.35 = bf16[4,4,1024,128]{3,2,1,0:T(8,128)(2,1)} copy(bf16[4,4,1024,128]{3,2,0,1:T(8,128)(2,1)} %bitcast.47) | data formatting | bytes 8388608 | tf_op jit(solution)/shard_map/transpose | solution.py:50
  266.3 6.4 %copy.36 = bf16[1024,16,128]{0,2,1:T(8,128)(2,1)} copy(bf16[1024,16,128]{2,0,1:T(8,128)(2,1)} %bitcast.45) | data formatting | bytes 8388608 | tf_op jit(solution)/shard_map/transpose | solution.py:14
  272.7 5.0 %copy.34 = bf16[4,4,128,1024]{3,2,1,0:T(8,128)(2,1)} copy(bf16[4,4,128,1024]{3,2,0,1:T(8,128)(2,1)} %bitcast.48) | data formatting | bytes 8388608 | tf_op jit(solution)/shard_map/transpose | solution.py:50
  277.7 22.9 %all-gather.13.cloned.1.call-done = bf16[1024,2048]{1,0:T(8,128)(2,1)} async-done(((bf16[1024,256]{1,0:T(8,128)(2,1)}), bf16[1024,2048]{1,0:T(8,128)(2,1)}) %all-gather.13.cloned.1.call-update) | async-done | bytes 4194320 | tf_op jit(solution)/shard_map/all_gather | solution.py:114
  300.6 3.1 fusion.3
  303.7 14.6 %convolution_convert_fusion.1 = bf16[1024,2048]{1,0:T(8,128)(2,1)} fusion(bf16[1024,2048]{0,1:T(8,128)(2,1)} %bitcast.49, bf16[2048,1024]{1,0:T(8,128)(2,1)} %bitcast.50, bf16[1024,2048]{1,0:T(8,128)(2,1)} %all-gather.13.cloned.1.call-done, f32[2048]{0:T(1024)S(1)} %convert_element_type.95, f32[1024]{0:T(1024)S(1)} %add_rsqrt_fusion.1), kind=kOutput, calls=%fused_computation.19 | convolution fusion | flops 8603566080 | bytes 16789504 | tf_op jit(solution)/shard_map/dot_general | solution.py:118
  318.3 2.5 copy.45
  320.8 52.6 %all_to_all.44 = bf16[8,1024,256]{2,1,0:T(8,128)(2,1)S(1)} all-to-all(bf16[8,1024,256]{2,1,0:T(8,128)(2,1)S(1)} %bitcast.46), channel_id=1, replica_groups=mesh['rep'=2,'fs_0'=4,'fs_1'=4,'tp'=8] {'tp'}, dimensions={0} | all-to-all | bytes 8388608 | tf_op jit(solution)/shard_map/all_to_all | solution.py:35
  373.4 0.6 convert_reduce_fusion
  374.0 0.2 multiply_reduce_fusion
  374.2 0.6 broadcast_in_dim.17
  374.8 4.3 %all-to-all-start.7 = ((f32[8,1,1024]{2,1,0:T(1,128)}), f32[8,1,1024]{2,1,0:T(1,128)S(1)}, u32[]{:S(2)}, u32[]{:S(2)}) async-start(f32[8,1,1024]{2,1,0:T(1,128)} %broadcast_in_dim.17), calls=%async_computation.7 | async-start | bytes 65536 | tf_op jit(solution)/shard_map/all_to_all | solution.py:21
  379.1 0.8 dynamic-slice_convert_fusion.1
  379.9 4.0 %all-to-all-done.7 = f32[8,1,1024]{2,1,0:T(1,128)S(1)} async-done(((f32[8,1,1024]{2,1,0:T(1,128)}), f32[8,1,1024]{2,1,0:T(1,128)S(1)}, u32[]{:S(2)}, u32[]{:S(2)}) %all-to-all-start.7) | async-done | bytes 32800 | tf_op jit(solution)/shard_map/all_to_all | solution.py:21
  383.9 1.1 add_convert_fusion
  (36 shorter events, 0.4 us)
Async XLA Ops:
  6.5 81.1 %copy-start.3 = (bf16[128,256]{1,0:T(8,128)(2,1)S(1)}, bf16[128,256]{1,0:T(8,128)(2,1)}, u32[]{:S(2)}) copy-start(bf16[128,256]{1,0:T(8,128)(2,1)} %param.16) | copy-start | bytes 196612
  6.5 39.2 %all-gather.19.cloned.1.call-start = ((), (), s32[]{:S(2)}) async-start(), calls=%async_computation.12 | async-start | bytes 1310720 | tf_op jit(solution)/shard_map/all_gather | solution.py:47
  7.3 91.2 %copy-start.5 = (bf16[256,128]{1,0:T(8,128)(2,1)S(1)}, bf16[256,128]{1,0:T(8,128)(2,1)}, u32[]{:S(2)}) copy-start(bf16[256,128]{1,0:T(8,128)(2,1)} %param.18) | copy-start | bytes 196612
  7.3 153.4 %all-gather.15.cloned.1.call-start = ((), (), s32[]{:S(2)}) async-start(), calls=%async_computation.10 | async-start | bytes 1310720 | tf_op jit(solution)/shard_map/all_gather | solution.py:47
  8.0 153.2 %all-gather.11.cloned.1.call-start = ((), (), s32[]{:S(2)}) async-start(), calls=%async_computation.8 | async-start | bytes 4718592 | tf_op jit(solution)/shard_map/all_gather | solution.py:90
  8.8 253.0 %all-gather.21.cloned.1.call-start = ((), (), s32[]{:S(2)}) async-start(), calls=%async_computation.13 | async-start | bytes 5242880 | tf_op jit(solution)/shard_map/all_gather | solution.py:47
  46.7 104.9 %copy-start.4 = (bf16[128,256]{1,0:T(8,128)(2,1)S(1)}, bf16[128,256]{1,0:T(8,128)(2,1)}, u32[]{:S(2)}) copy-start(bf16[128,256]{1,0:T(8,128)(2,1)} %param.14) | copy-start | bytes 196612
  88.7 72.0 %copy-start.6 = (bf16[2048]{0:T(1024)(128)(2,1)S(1)}, bf16[2048]{0:T(1024)(128)(2,1)}, u32[]{:S(2)}) copy-start(bf16[2048]{0:T(1024)(128)(2,1)} %param.13) | copy-start | bytes 12292
  88.7 31.8 %all-to-all-start.2 = ((bf16[16,128,256]{2,1,0:T(8,128)(2,1)}), bf16[16,128,256]{2,1,0:T(8,128)(2,1)S(1)}, u32[]{:S(2)}, u32[]{:S(2)}) async-start(bf16[16,128,256]{2,1,0:T(8,128)(2,1)} %broadcast_in_dim.14), calls=%async_computation.2 | async-start | bytes 2097152 | tf_op jit(solution)/shard_map/all_to_all | solution.py:21
  121.5 30.1 %all-to-all-start.3 = ((bf16[16,256,128]{1,2,0:T(8,128)(2,1)}), bf16[16,256,128]{1,2,0:T(8,128)(2,1)S(1)}, u32[]{:S(2)}, u32[]{:S(2)}) async-start(bf16[16,256,128]{1,2,0:T(8,128)(2,1)} %broadcast_in_dim.15), calls=%async_computation.3 | async-start | bytes 2097152 | tf_op jit(solution)/shard_map/all_to_all | solution.py:21
  152.8 30.1 %all-to-all-start = ((bf16[16,128,256]{2,1,0:T(8,128)(2,1)}), bf16[16,128,256]{2,1,0:T(8,128)(2,1)}, u32[]{:S(2)}, u32[]{:S(2)}) async-start(bf16[16,128,256]{2,1,0:T(8,128)(2,1)} %broadcast_in_dim.12), calls=%async_computation | async-start | bytes 2097152 | tf_op jit(solution)/shard_map/all_to_all | solution.py:21
  160.6 112.1 %all-gather.17.cloned.1.call-start = ((), (), s32[]{:S(2)}) async-start(), calls=%async_computation.11 | async-start | bytes 5242880 | tf_op jit(solution)/shard_map/all_gather | solution.py:47
  161.2 3.5 copy-start.1
  250.2 10.5 %copy-start.2 = (bf16[1024,256]{1,0:T(8,128)(2,1)S(1)}, bf16[1024,256]{1,0:T(8,128)(2,1)}, u32[]{:S(2)}) copy-start(bf16[1024,256]{1,0:T(8,128)(2,1)} %param.12) | copy-start | bytes 1572868
  250.2 11.5 %copy-start.7 = (bf16[2048]{0:T(1024)(128)(2,1)S(1)}, bf16[2048]{0:T(1024)(128)(2,1)}, u32[]{:S(2)}) copy-start(bf16[2048]{0:T(1024)(128)(2,1)} %param.20) | copy-start | bytes 12292
  251.6 9.0 %all-to-all-start.5 = ((f32[8,1,1024]{2,1,0:T(1,128)}), f32[8,1,1024]{2,1,0:T(1,128)S(1)}, u32[]{:S(2)}, u32[]{:S(2)}) async-start(f32[8,1,1024]{2,1,0:T(1,128)} %broadcast_in_dim.16), calls=%async_computation.5 | async-start | bytes 65536 | tf_op jit(solution)/shard_map/all_to_all | solution.py:21
  255.8 44.7 %all-gather.13.cloned.1.call-start = ((), (), s32[]{:S(2)}) async-start(), calls=%async_computation.9 | async-start | bytes 4718592 | tf_op jit(solution)/shard_map/all_gather | solution.py:114
  373.4 10.5 %copy-start = (bf16[1024,256]{1,0:T(8,128)(2,1)S(1)}, bf16[1024,256]{1,0:T(8,128)(2,1)}, u32[]{:S(2)}) copy-start(bf16[1024,256]{1,0:T(8,128)(2,1)} %add_convert_fusion.1) | copy-start | bytes 1572868
  374.8 9.0 %all-to-all-start.7 = ((f32[8,1,1024]{2,1,0:T(1,128)}), f32[8,1,1024]{2,1,0:T(1,128)S(1)}, u32[]{:S(2)}, u32[]{:S(2)}) async-start(f32[8,1,1024]{2,1,0:T(1,128)} %broadcast_in_dim.17), calls=%async_computation.7 | async-start | bytes 65536 | tf_op jit(solution)/shard_map/all_to_all | solution.py:21
Sparse Core Ops, SparseCore 0:
  9.1 36.5 all-gather.18
  47.5 43.0 all-gather.14
  92.5 42.0 all-gather.10
  136.3 62.9 all-gather.20
  200.9 51.1 all-gather.16
  261.8 38.7 all-gather.12
where the time goes:
time: 393 us; the launch traced here: 392 us
  blocking collectives  150 us (38%)
  waiting for transfers between devices  129 us (33%)
  starting transfers between devices  34.2 us (9%)
  local copies, waits for them, and re-layouts  26.7 us (7%)
  matrix products  26.1 us (7%)
  between operations  13.7 us (3%)
  other arithmetic  12.6 us (3%)
    all_to_all x2, blocking collectives, sent_and_summed(): lax.all_to_all(pieces, axis, split_axis=0, concat_axis=0, tiled=True)  109 us
    all_to_all x5, waiting for transfers between devices, from_everyone(): lax.all_to_all(jnp.broadcast_to(x[None], (length, *x.shape)), axis, 0, 0,...  66.4 us
    all_to_all x1, blocking collectives, from_everyone(): lax.all_to_all(jnp.broadcast_to(x[None], (length, *x.shape)), axis, 0, 0,...  40.9 us
    all_gather x4, waiting for transfers between devices, all_blocks(): pieces = lax.all_gather(pieces, axes[k])  37 us
    all_to_all x5, starting transfers between devices, from_everyone(): lax.all_to_all(jnp.broadcast_to(x[None], (length, *x.shape)), axis, 0, 0,...  34 us
    all_gather x1, waiting for transfers between devices, body(): resid = lax.all_gather(resid_own, 'tp', axis=1, tiled=True)  22.9 us
    dot_general x1, matrix products, body(): jnp.dot(active, whole_of(down_weight, FS, (0, 1), 1), preferred_element_t...  14.6 us
    transpose x2, local copies, waits for them, and re-layouts, all_blocks(): pieces = pieces.transpose(*back, *range(len(axes), pieces.ndim))  9.5 us
  transfers between devices with their start and end apart: 11, of which 7 were waited for; matrix products, arithmetic and copies ran while one was open for 11% of the time, Pallas kernels for 0%

commit v1 on v0

--- a/solution.py
+++ b/solution.py
@@ -111,7 +111,10 @@
     gain_own = lax.dynamic_slice_in_dim(mix_out_gain, first, own_width, 0).astype(jnp.float32)
     scaled = mixed * lax.rsqrt(power[:, None] / full_width + epsilon) * gain_own
     resid_own = (tokens.astype(jnp.float32) + scaled).astype(jnp.bfloat16)
-    resid = lax.all_gather(resid_own, "tp", axis=1, tiled=True)
+    size = lax.axis_size("tp")
+    shards = jnp.stack([resid_own for _ in range(size)])
+    shards = lax.all_to_all(shards, "tp", split_axis=0, concat_axis=0)
+    resid = jnp.concatenate(shards, axis=1)
     second = normalize(resid, ffn_in_gain).astype(jnp.bfloat16)
     lifted = jnp.dot(second, whole_of(up_weight, FS, (0, 1), 0), preferred_element_type=jnp.float32)
     active = jnp.square(jnp.maximum(lifted, 0.0)).astype(jnp.bfloat16)

time: 393 us -> 397 us (1.010)
  blocking collectives: 150 us -> 97.9 us
  starting transfers between devices: 34.2 us -> 61.6 us
  waiting for transfers between devices: 129 us -> 146 us
  other arithmetic: 12.6 us -> 18.3 us
  local copies, waits for them, and re-layouts: 26.7 us -> 31.9 us
    all_to_all x0 -> x2, waiting for transfers between devices: none -> 81.3 us  [the longest x1 48.2 us: sent_and_summed(): lax.all_to_all(pieces, axis, split_axis=0, concat_axis=0, tiled=True)]
    all_to_all x2 -> x1, blocking collectives: 109 us -> 52.1 us  [sent_and_summed(): lax.all_to_all(pieces, axis, split_axis=0, concat_axis=0, tiled=True)]
    all_gather x4, waiting for transfers between devices: 37 us -> 0.05 us  [all_blocks(): pieces = lax.all_gather(pieces, axes[k])]
    all_gather x1 -> x0, waiting for transfers between devices: 22.9 us -> none  [body(): resid = lax.all_gather(resid_own, 'tp', axis=1, tiled=True)]
    all_to_all x0 -> x2, starting transfers between devices: none -> 18.7 us  [the longest x1 13.4 us: sent_and_summed(): lax.all_to_all(pieces, axis, split_axis=0, concat_axis=0, tiled=True)]
    all_to_all x5, starting transfers between devices: 34 us -> 42.8 us  [from_everyone(): lax.all_to_all(jnp.broadcast_to(x[None], (length, *x.shape)), axis, 0, 0,...]
    all_to_all x1, blocking collectives: 40.9 us -> 45.8 us  [from_everyone(): lax.all_to_all(jnp.broadcast_to(x[None], (length, *x.shape)), axis, 0, 0,...]
    all_to_all x5, waiting for transfers between devices: 66.4 us -> 61.7 us  [from_everyone(): lax.all_to_all(jnp.broadcast_to(x[None], (length, *x.shape)), axis, 0, 0,...]
  transfers between devices with their start and end apart: 11 -> 12, of which waited for: 7 -> 7; matrix products, arithmetic and copies ran while one was open for 11% -> 13% of each run, Pallas kernels for 0% -> 0%
where the time goes in v1:
time: 397 us; the launch traced here: 395 us
  waiting for transfers between devices  146 us (37%)
  blocking collectives  97.9 us (25%)
  starting transfers between devices  61.6 us (16%)
  local copies, waits for them, and re-layouts  31.9 us (8%)
  matrix products  26.2 us (7%)
  other arithmetic  18.3 us (5%)
  between operations  13.4 us (3%)
    all_to_all x5, waiting for transfers between devices, from_everyone(): lax.all_to_all(jnp.broadcast_to(x[None], (length, *x.shape)), axis, 0, 0,...  61.7 us
    all_to_all x1, blocking collectives, sent_and_summed(): lax.all_to_all(pieces, axis, split_axis=0, concat_axis=0, tiled=True)  52.1 us
    all_to_all x1, waiting for transfers between devices, sent_and_summed(): lax.all_to_all(pieces, axis, split_axis=0, concat_axis=0, tiled=True)  48.2 us
    all_to_all x1, blocking collectives, from_everyone(): lax.all_to_all(jnp.broadcast_to(x[None], (length, *x.shape)), axis, 0, 0,...  45.8 us
    all_to_all x5, starting transfers between devices, from_everyone(): lax.all_to_all(jnp.broadcast_to(x[None], (length, *x.shape)), axis, 0, 0,...  42.8 us
    all_to_all x1, waiting for transfers between devices, body(): shards = lax.all_to_all(shards, 'tp', split_axis=0, concat_axis=0)  33.1 us
    dot_general x1, matrix products, body(): jnp.dot(active, whole_of(down_weight, FS, (0, 1), 1), preferred_element_t...  14.4 us
    all_to_all x1, starting transfers between devices, sent_and_summed(): lax.all_to_all(pieces, axis, split_axis=0, concat_axis=0, tiled=True)  13.4 us
  transfers between devices with their start and end apart: 12, of which 7 were waited for; matrix products, arithmetic and copies ran while one was open for 13% of the time, Pallas kernels for 0%

profile of v1, /device:TPU:1, one launch (start us, length us, event | category | flops | bytes accessed | tf_op | source)
XLA Modules:
  0.0 395.4 jit_solution(11568937748411543078)
XLA Ops:
  6.5 0.7 all-gather.16.cloned.1.call-update
  7.3 0.7 all-gather.10.cloned.1.call-update
  8.0 0.9 broadcast_in_dim.13
  8.9 45.8 %all_to_all.47 = bf16[16,128,256]{2,1,0:T(8,128)(2,1)S(1)} all-to-all(bf16[16,128,256]{2,1,0:T(8,128)(2,1)S(1)} %broadcast_in_dim.13), channel_id=1, replica_groups=mesh['rep'=2,'fs_0'=4,'fs_1'=4,'tp'=8] {'fs_0','fs_1'}, dimensions={0} | all-to-all | bytes 2097152 | tf_op jit(solution)/shard_map/all_to_all | solution.py:21
  54.7 2.0 broadcast_in_dim.14
  56.7 9.1 %all-to-all-start.2 = ((bf16[16,128,256]{2,1,0:T(8,128)(2,1)}), bf16[16,128,256]{2,1,0:T(8,128)(2,1)S(1)}, u32[]{:S(2)}, u32[]{:S(2)}) async-start(bf16[16,128,256]{2,1,0:T(8,128)(2,1)} %broadcast_in_dim.14), calls=%async_computation.2 | async-start | bytes 2097152 | tf_op jit(solution)/shard_map/all_to_all | solution.py:21
  65.9 0.7 all-gather.12.cloned.1.call-update
  66.7 21.3 %all-to-all-done.2 = bf16[16,128,256]{2,1,0:T(8,128)(2,1)S(1)} async-done(((bf16[16,128,256]{2,1,0:T(8,128)(2,1)}), bf16[16,128,256]{2,1,0:T(8,128)(2,1)S(1)}, u32[]{:S(2)}, u32[]{:S(2)}) %all-to-all-start.2) | async-done | bytes 1048608 | tf_op jit(solution)/shard_map/all_to_all | solution.py:21
  88.0 1.1 broadcast_in_dim.15
  89.1 7.9 %all-to-all-start.3 = ((bf16[16,256,128]{1,2,0:T(8,128)(2,1)}), bf16[16,256,128]{1,2,0:T(8,128)(2,1)S(1)}, u32[]{:S(2)}, u32[]{:S(2)}) async-start(bf16[16,256,128]{1,2,0:T(8,128)(2,1)} %broadcast_in_dim.15), calls=%async_computation.3 | async-start | bytes 2097152 | tf_op jit(solution)/shard_map/all_to_all | solution.py:21
  97.0 0.5 all-gather.18.cloned.1.call-update
  97.6 0.7 dynamic-slice_convert_fusion
  98.2 20.9 %all-to-all-done.3 = bf16[16,256,128]{1,2,0:T(8,128)(2,1)S(1)} async-done(((bf16[16,256,128]{1,2,0:T(8,128)(2,1)}), bf16[16,256,128]{1,2,0:T(8,128)(2,1)S(1)}, u32[]{:S(2)}, u32[]{:S(2)}) %all-to-all-start.3) | async-done | bytes 1048608 | tf_op jit(solution)/shard_map/all_to_all | solution.py:21
  119.1 1.1 broadcast_in_dim.12
  120.2 17.2 %all-to-all-start = ((bf16[16,128,256]{2,1,0:T(8,128)(2,1)}), bf16[16,128,256]{2,1,0:T(8,128)(2,1)}, u32[]{:S(2)}, u32[]{:S(2)}) async-start(bf16[16,128,256]{2,1,0:T(8,128)(2,1)} %broadcast_in_dim.12), calls=%async_computation | async-start | bytes 2097152 | tf_op jit(solution)/shard_map/all_to_all | solution.py:21
  137.6 3.2 fusion
  141.0 1.3 fusion.8
  142.3 1.3 fusion.7
  143.6 0.3 multiply_add_fusion
  143.9 11.6 %all-to-all-done = bf16[16,128,256]{2,1,0:T(8,128)(2,1)} async-done(((bf16[16,128,256]{2,1,0:T(8,128)(2,1)}), bf16[16,128,256]{2,1,0:T(8,128)(2,1)}, u32[]{:S(2)}, u32[]{:S(2)}) %all-to-all-start) | async-done | bytes 1048608 | tf_op jit(solution)/shard_map/all_to_all | solution.py:21
  155.5 9.2 %convolution_convert_fusion = bf16[1024,2048]{1,0:T(8,128)(2,1)} fusion(bf16[256,2048]{0,1:T(8,128)(2,1)S(1)} %bitcast.62, f32[1024,256]{1,0:T(8,128)S(1)} %bitcast.63, bf16[2048,256]{1,0:T(8,128)(2,1)} %bitcast, bf16[1024,2048]{1,0:T(8,128)(2,1)} %all-gather.10.cloned.1.call-done, f32[2048]{0:T(1024)S(1)} %convert_element_type.86, ...), kind=kOutput, calls=%fused_computation.15 | convolution fusion | flops 2159017984 | bytes 11546624 | tf_op jit(solution)/shard_map/dot_general | solution.py:106
  164.7 4.4 %copy.51 = bf16[128,8,8,256]{3,2,0,1:T(8,128)(2,1)} copy(bf16[128,8,8,256]{3,2,1,0:T(8,128)(2,1)} %bitcast.55) | data formatting | bytes 8388608 | tf_op jit(solution)/shard_map/reshape | solution.py:30
  169.1 13.4 %all-to-all-start.4 = ((bf16[8,1024,256]{2,1,0:T(8,128)(2,1)}), bf16[8,1024,256]{2,1,0:T(8,128)(2,1)}, u32[]{:S(2)}, u32[]{:S(2)}) async-start(bf16[8,1024,256]{2,1,0:T(8,128)(2,1)} %bitcast.48), calls=%async_computation.4 | async-start | bytes 8388608 | tf_op jit(solution)/shard_map/all_to_all | solution.py:35
  182.5 0.5 all-gather.14.cloned.1.call-update
  183.0 48.2 %all-to-all-done.4 = bf16[8,1024,256]{2,1,0:T(8,128)(2,1)} async-done(((bf16[8,1024,256]{2,1,0:T(8,128)(2,1)}), bf16[8,1024,256]{2,1,0:T(8,128)(2,1)}, u32[]{:S(2)}, u32[]{:S(2)}) %all-to-all-start.4) | async-done | bytes 4194336 | tf_op jit(solution)/shard_map/all_to_all | solution.py:35
  231.2 2.9 convert_reduce_fusion.1
  234.4 0.6 broadcast_in_dim.16
  235.0 4.2 %all-to-all-start.5 = ((f32[8,1,1024]{2,1,0:T(1,128)}), f32[8,1,1024]{2,1,0:T(1,128)S(1)}, u32[]{:S(2)}, u32[]{:S(2)}) async-start(f32[8,1,1024]{2,1,0:T(1,128)} %broadcast_in_dim.16), calls=%async_computation.5 | async-start | bytes 65536 | tf_op jit(solution)/shard_map/all_to_all | solution.py:21
  239.2 0.8 dynamic-slice_convert_fusion.2
  240.0 4.0 %all-to-all-done.5 = f32[8,1,1024]{2,1,0:T(1,128)S(1)} async-done(((f32[8,1,1024]{2,1,0:T(1,128)}), f32[8,1,1024]{2,1,0:T(1,128)S(1)}, u32[]{:S(2)}, u32[]{:S(2)}) %all-to-all-start.5) | async-done | bytes 32800 | tf_op jit(solution)/shard_map/all_to_all | solution.py:21
  244.1 0.3 add_convert_fusion.1
  244.6 2.5 stack.2
  247.0 5.3 %all-to-all-start.6 = ((bf16[8,1024,256]{1,2,0:T(8,128)(2,1)}), bf16[8,1024,256]{1,2,0:T(8,128)(2,1)}, u32[]{:S(2)}, u32[]{:S(2)}) async-start(bf16[8,1024,256]{1,2,0:T(8,128)(2,1)} %stack.2), calls=%async_computation.6 | async-start | bytes 8388608 | tf_op jit(solution)/shard_map/all_to_all | solution.py:116
  252.3 4.5 %copy.40 = bf16[4,4,1024,128]{3,2,1,0:T(8,128)(2,1)} copy(bf16[4,4,1024,128]{3,2,0,1:T(8,128)(2,1)} %bitcast.51) | data formatting | bytes 8388608 | tf_op jit(solution)/shard_map/transpose | solution.py:50
  256.9 6.4 %copy.41 = bf16[1024,16,128]{0,2,1:T(8,128)(2,1)} copy(bf16[1024,16,128]{2,0,1:T(8,128)(2,1)} %bitcast.49) | data formatting | bytes 8388608 | tf_op jit(solution)/shard_map/transpose | solution.py:14
  263.3 4.7 %copy.39 = bf16[4,4,128,1024]{3,2,1,0:T(8,128)(2,1)} copy(bf16[4,4,128,1024]{3,2,0,1:T(8,128)(2,1)} %bitcast.52) | data formatting | bytes 8388608 | tf_op jit(solution)/shard_map/transpose | solution.py:50
  268.0 33.1 %all-to-all-done.6 = bf16[8,1024,256]{1,2,0:T(8,128)(2,1)} async-done(((bf16[8,1024,256]{1,2,0:T(8,128)(2,1)}), bf16[8,1024,256]{1,2,0:T(8,128)(2,1)}, u32[]{:S(2)}, u32[]{:S(2)}) %all-to-all-start.6) | async-done | bytes 4194336 | tf_op jit(solution)/shard_map/all_to_all | solution.py:116
  301.1 3.1 fusion.3
  304.2 4.1 %fusion.5 = bf16[8,1024,256]{1,2,0:T(8,128)(2,1)} fusion(bf16[8,1024,256]{1,2,0:T(8,128)(2,1)} %all-to-all-done.6, f32[8,256]{1,0:T(8,128)S(1)} %reshape.111, f32[1024]{0:T(1024)S(1)} %add_rsqrt_fusion.1), kind=kLoop, calls=%fused_computation.9 | loop fusion | flops 8388608 | bytes 8400896 | tf_op jit(solution)/shard_map/convert_element_type | solution.py:118
  308.3 14.4 %convolution_convert_fusion.1 = bf16[1024,2048]{1,0:T(8,128)(2,1)} fusion(bf16[1024,2048]{0,1:T(8,128)(2,1)} %bitcast.53, bf16[1024,2048]{0,1:T(8,128)(2,1)} %bitcast.56, bf16[2048,1024]{1,0:T(8,128)(2,1)} %bitcast.54), kind=kOutput, calls=%fused_computation.16 | convolution fusion | flops 8595177472 | bytes 16777216 | tf_op jit(solution)/shard_map/dot_general | solution.py:121
  322.7 2.5 copy.50
  325.2 52.1 %all_to_all.48 = bf16[8,1024,256]{2,1,0:T(8,128)(2,1)S(1)} all-to-all(bf16[8,1024,256]{2,1,0:T(8,128)(2,1)S(1)} %bitcast.50), channel_id=1, replica_groups=mesh['rep'=2,'fs_0'=4,'fs_1'=4,'tp'=8] {'tp'}, dimensions={0} | all-to-all | bytes 8388608 | tf_op jit(solution)/shard_map/all_to_all | solution.py:35
  377.3 0.6 convert_reduce_fusion
  378.1 0.6 broadcast_in_dim.17
  378.7 4.3 %all-to-all-start.8 = ((f32[8,1,1024]{2,1,0:T(1,128)}), f32[8,1,1024]{2,1,0:T(1,128)S(1)}, u32[]{:S(2)}, u32[]{:S(2)}) async-start(f32[8,1,1024]{2,1,0:T(1,128)} %broadcast_in_dim.17), calls=%async_computation.8 | async-start | bytes 65536 | tf_op jit(solution)/shard_map/all_to_all | solution.py:21
  383.0 0.8 dynamic-slice_convert_fusion.1
  383.7 4.0 %all-to-all-done.8 = f32[8,1,1024]{2,1,0:T(1,128)S(1)} async-done(((f32[8,1,1024]{2,1,0:T(1,128)}), f32[8,1,1024]{2,1,0:T(1,128)S(1)}, u32[]{:S(2)}, u32[]{:S(2)}) %all-to-all-start.8) | async-done | bytes 32800 | tf_op jit(solution)/shard_map/all_to_all | solution.py:21
  387.8 1.1 add_convert_fusion
  (35 shorter events, 1.3 us)
Async XLA Ops:
  6.5 60.1 %copy-start.3 = (bf16[256,128]{1,0:T(8,128)(2,1)S(1)}, bf16[256,128]{1,0:T(8,128)(2,1)}, u32[]{:S(2)}) copy-start(bf16[256,128]{1,0:T(8,128)(2,1)} %param.18) | copy-start | bytes 196612
  6.5 90.5 %all-gather.16.cloned.1.call-start = ((), (), s32[]{:S(2)}) async-start(), calls=%async_computation.12 | async-start | bytes 1310720 | tf_op jit(solution)/shard_map/all_gather | solution.py:47
  7.3 130.3 %all-gather.10.cloned.1.call-start = ((), (), s32[]{:S(2)}) async-start(), calls=%async_computation.9 | async-start | bytes 4718592 | tf_op jit(solution)/shard_map/all_gather | solution.py:90
  54.7 64.4 %copy-start.2 = (bf16[128,256]{1,0:T(8,128)(2,1)S(1)}, bf16[128,256]{1,0:T(8,128)(2,1)}, u32[]{:S(2)}) copy-start(bf16[128,256]{1,0:T(8,128)(2,1)} %param.14) | copy-start | bytes 196612
  56.7 31.3 %all-to-all-start.2 = ((bf16[16,128,256]{2,1,0:T(8,128)(2,1)}), bf16[16,128,256]{2,1,0:T(8,128)(2,1)S(1)}, u32[]{:S(2)}, u32[]{:S(2)}) async-start(bf16[16,128,256]{2,1,0:T(8,128)(2,1)} %broadcast_in_dim.14), calls=%async_computation.2 | async-start | bytes 2097152 | tf_op jit(solution)/shard_map/all_to_all | solution.py:21
  65.9 71.6 %copy-start.4 = (bf16[2048]{0:T(1024)(128)(2,1)S(1)}, bf16[2048]{0:T(1024)(128)(2,1)}, u32[]{:S(2)}) copy-start(bf16[2048]{0:T(1024)(128)(2,1)} %param.13) | copy-start | bytes 12292
  65.9 116.6 %all-gather.12.cloned.1.call-start = ((), (), s32[]{:S(2)}) async-start(), calls=%async_computation.10 | async-start | bytes 1310720 | tf_op jit(solution)/shard_map/all_gather | solution.py:47
  89.1 30.1 %all-to-all-start.3 = ((bf16[16,256,128]{1,2,0:T(8,128)(2,1)}), bf16[16,256,128]{1,2,0:T(8,128)(2,1)S(1)}, u32[]{:S(2)}, u32[]{:S(2)}) async-start(bf16[16,256,128]{1,2,0:T(8,128)(2,1)} %broadcast_in_dim.15), calls=%async_computation.3 | async-start | bytes 2097152 | tf_op jit(solution)/shard_map/all_to_all | solution.py:21
  97.0 155.3 %all-gather.18.cloned.1.call-start = ((), (), s32[]{:S(2)}) async-start(), calls=%async_computation.13 | async-start | bytes 5242880 | tf_op jit(solution)/shard_map/all_gather | solution.py:47
  120.2 35.3 %all-to-all-start = ((bf16[16,128,256]{2,1,0:T(8,128)(2,1)}), bf16[16,128,256]{2,1,0:T(8,128)(2,1)}, u32[]{:S(2)}, u32[]{:S(2)}) async-start(bf16[16,128,256]{2,1,0:T(8,128)(2,1)} %broadcast_in_dim.12), calls=%async_computation | async-start | bytes 2097152 | tf_op jit(solution)/shard_map/all_to_all | solution.py:21
  137.5 3.5 copy-start
  169.1 62.2 %all-to-all-start.4 = ((bf16[8,1024,256]{2,1,0:T(8,128)(2,1)}), bf16[8,1024,256]{2,1,0:T(8,128)(2,1)}, u32[]{:S(2)}, u32[]{:S(2)}) async-start(bf16[8,1024,256]{2,1,0:T(8,128)(2,1)} %bitcast.48), calls=%async_computation.4 | async-start | bytes 8388608 | tf_op jit(solution)/shard_map/all_to_all | solution.py:35
  182.5 61.6 %copy-start.1 = (bf16[1024,256]{1,0:T(8,128)(2,1)S(1)}, bf16[1024,256]{1,0:T(8,128)(2,1)}, u32[]{:S(2)}) copy-start(bf16[1024,256]{1,0:T(8,128)(2,1)} %param.12) | copy-start | bytes 1572868
  182.5 80.8 %all-gather.14.cloned.1.call-start = ((), (), s32[]{:S(2)}) async-start(), calls=%async_computation.11 | async-start | bytes 5242880 | tf_op jit(solution)/shard_map/all_gather | solution.py:47
  235.0 9.0 %all-to-all-start.5 = ((f32[8,1,1024]{2,1,0:T(1,128)}), f32[8,1,1024]{2,1,0:T(1,128)S(1)}, u32[]{:S(2)}, u32[]{:S(2)}) async-start(f32[8,1,1024]{2,1,0:T(1,128)} %broadcast_in_dim.16), calls=%async_computation.5 | async-start | bytes 65536 | tf_op jit(solution)/shard_map/all_to_all | solution.py:21
  247.0 5.3 %copy-start.5 = (bf16[2048]{0:T(1024)(128)(2,1)S(1)}, bf16[2048]{0:T(1024)(128)(2,1)}, u32[]{:S(2)}) copy-start(bf16[2048]{0:T(1024)(128)(2,1)} %param.20) | copy-start | bytes 12292
  247.0 54.1 %all-to-all-start.6 = ((bf16[8,1024,256]{1,2,0:T(8,128)(2,1)}), bf16[8,1024,256]{1,2,0:T(8,128)(2,1)}, u32[]{:S(2)}, u32[]{:S(2)}) async-start(bf16[8,1024,256]{1,2,0:T(8,128)(2,1)} %stack.2), calls=%async_computation.6 | async-start | bytes 8388608 | tf_op jit(solution)/shard_map/all_to_all | solution.py:116
  378.7 9.0 %all-to-all-start.8 = ((f32[8,1,1024]{2,1,0:T(1,128)}), f32[8,1,1024]{2,1,0:T(1,128)S(1)}, u32[]{:S(2)}, u32[]{:S(2)}) async-start(f32[8,1,1024]{2,1,0:T(1,128)} %broadcast_in_dim.17), calls=%async_computation.8 | async-start | bytes 65536 | tf_op jit(solution)/shard_map/all_to_all | solution.py:21
Sparse Core Ops, SparseCore 0:
  9.1 47.4 all-gather.15
  58.4 41.5 all-gather.9
  101.9 37.4 all-gather.11
  141.0 52.7 all-gather.17
  195.5 52.1 all-gather.13
